TPU v7x, 32 devices: a whole 2x2x4 slice. The times are simulated.
32 devices in a mesh: ep: 16 (over z, y, x), tp: 2 (over core).
Axes of the slice: x: 2, y: 2, z: 4, core: 2. Of those that a mesh axis runs over, the one named last changes fastest.
Arguments:
- tokens: bfloat16 [128, 2048], P('ep'), may hold values from -6 to 6
- mixer_norm_gain: float32 [2048], replicated, may hold values from 0.1 to 1.9
- gate_projection_weight: bfloat16 [2048, 2, 2048], P(None, 'tp', 'ep'), may hold values from -0.125 to 0.125
- value_projection_weight: bfloat16 [2048, 2, 2048], P(None, 'tp', 'ep'), may hold values from -0.125 to 0.125
- input_projection_weight: bfloat16 [2048, 1024], P(None, 'tp'), may hold values from -0.125 to 0.125
- output_projection_weight: bfloat16 [2048, 1024], P(None, 'tp'), may hold values from -0.125 to 0.125
- step_projection_weight: bfloat16 [2048, 64], P(None, 'tp'), may hold values from -0.125 to 0.125
- head_step_bias: float32 [64], P('tp'), may hold values from -1 to 1
- head_decay_rate: float32 [64], P('tp'), may hold values from 0.02 to 3
- extra_log_decay: float32 [128, 64], P('ep', 'tp'), may hold values from -0.7 to 0
- value_taps: float32 [4, 4096], P(None, 'tp'), may hold values from -3 to 3
- input_taps: float32 [4, 1024], P(None, 'tp'), may hold values from -3 to 3
- output_taps: float32 [4, 1024], P(None, 'tp'), may hold values from -3 to 3
- prior_values: bfloat16 [128, 3, 4096], P('ep', None, 'tp'), may hold values from -6 to 6
- prior_input_maps: bfloat16 [128, 3, 1024], P('ep', None, 'tp'), may hold values from -6 to 6
- prior_output_maps: bfloat16 [128, 3, 1024], P('ep', None, 'tp'), may hold values from -6 to 6
- head_skip_gain: float32 [64], P('tp'), may hold values from 0.5 to 1.5
- group_norm_gain: float32 [4096], P('tp'), may hold values from 0.1 to 1.9
- mixer_output_weight: bfloat16 [4096, 2048], P('tp', 'ep'), may hold values from -0.09375 to 0.09375
- recurrent_state: float32 [128, 64, 64, 128], P('ep', 'tp'), may hold values from -6 to 6
- expert_norm_gain: float32 [2048], replicated, may hold values from 0.1 to 1.9
- routes: int32 [128, 6], P('ep'), may hold values from 0 to 15, all different within a row; in each aligned block of 8 rows (0 to 7, 8 to 15, ...) at most 4 rows name the same one
- chosen_expert_weight: float32 [128, 6], P('ep'), may hold values from 0.2 to 1
- routed_gate_weight: bfloat16 [16, 2048, 512], P('ep', None, 'tp'), may hold values from -0.125 to 0.125
- routed_up_weight: bfloat16 [16, 2048, 512], P('ep', None, 'tp'), may hold values from -0.125 to 0.125
- routed_down_weight: bfloat16 [16, 512, 2048], P('ep', 'tp'), may hold values from -0.25 to 0.25
- common_gate_weight: bfloat16 [2048, 512], P(None, 'tp'), may hold values from -0.125 to 0.125
- common_up_weight: bfloat16 [2048, 512], P(None, 'tp'), may hold values from -0.125 to 0.125
- common_down_weight: bfloat16 [512, 2048], P('tp'), may hold values from -0.25 to 0.25
Outputs:
- result: bfloat16 [128, 2048], P('ep')
- state_next: float32 [128, 64, 64, 128], P('ep', 'tp')
- next_value: bfloat16 [128, 3, 4096], P('ep', None, 'tp')
- next_input: bfloat16 [128, 3, 1024], P('ep', None, 'tp')
- next_output: bfloat16 [128, 3, 1024], P('ep', None, 'tp')
Inputs may be any that keep to these rules, and one draw needn't show every extreme that they name: `routes`: the 6 experts of a row differ; among the rows of one device (aligned blocks of 8 rows) no expert is named more than 4 times.
All inputs are finite; a program needn't handle non-finite values.
Results may differ from a plain program's by a relative error of at most 0.015.
Values may be sent and summed in bfloat16 or wider, within the bound.
No kernel may reach another device: no remote copies, remote signals or barrier semaphores. Data moves between devices by JAX's collectives and lax.ppermute only.
A program may use at most 128 MiB of HBM per device.

v0:
```python
import jax
import jax.numpy as jnp
from jax import lax
from jax.sharding import PartitionSpec as P

D_INNER = 4096
GROUPS = 8
EPSILON = 1e-06


def rms_scale(values, gain_vec):
    values = values.astype(jnp.float32)
    return (
        values * lax.rsqrt(jnp.mean(values * values, axis=-1, keepdims=True) + EPSILON) * gain_vec
    )


def short_conv(past_rows, fresh_row, weight):
    window = jnp.concatenate([past_rows, fresh_row[:, None, :]], axis=1)
    summed = window[:, 0].astype(jnp.float32) * weight[0]
    for offset in range(1, window.shape[1]):
        summed = summed + window[:, offset].astype(jnp.float32) * weight[offset]
    return (jax.nn.silu(summed), window[:, 1:])


def state_step(
    state_prev, value_conv, input_conv, output_conv, timestep_size, step_decay, head_skip_gain
):
    batch_rows, head_count, head_size, state_size = state_prev.shape
    per_group = head_count // (input_conv.shape[1] // state_size)
    value_heads = value_conv.reshape(batch_rows, head_count, head_size)
    input_heads = jnp.repeat(input_conv.reshape(batch_rows, -1, state_size), per_group, axis=1)
    output_heads = jnp.repeat(output_conv.reshape(batch_rows, -1, state_size), per_group, axis=1)
    state_next = (
        step_decay[:, :, None, None] * state_prev
        + (timestep_size[:, :, None] * value_heads)[:, :, :, None] * input_heads[:, :, None, :]
    )
    mixed_heads = (
        jnp.sum(state_next * output_heads[:, :, None, :], axis=-1)
        + head_skip_gain[None, :, None] * value_heads
    )
    return (state_next, mixed_heads.reshape(batch_rows, -1))


def gated_norm(mixed_flat, gate_rows, group_norm_gain, group_width):
    gated_rows = mixed_flat * jax.nn.silu(gate_rows.astype(jnp.float32))
    grouped = gated_rows.reshape(gated_rows.shape[0], -1, group_width)
    grouped = grouped * lax.rsqrt(jnp.mean(grouped * grouped, axis=-1, keepdims=True) + EPSILON)
    return (grouped.reshape(gated_rows.shape[0], -1) * group_norm_gain).astype(jnp.bfloat16)


def expert_partial(arrived, gate_mat, up_mat, down_mat):
    gate_part = jnp.einsum("slcd,ldf->slcf", arrived, gate_mat, preferred_element_type=jnp.float32)
    up_part = jnp.einsum("slcd,ldf->slcf", arrived, up_mat, preferred_element_type=jnp.float32)
    hidden = (jax.nn.silu(gate_part) * up_part).astype(jnp.bfloat16)
    return jnp.einsum("slcf,lfd->slcd", hidden, down_mat, preferred_element_type=jnp.float32)


def shards(
    tokens,
    mixer_norm_gain,
    gate_projection_weight,
    value_projection_weight,
    input_projection_weight,
    output_projection_weight,
    step_projection_weight,
    head_step_bias,
    head_decay_rate,
    extra_log_decay,
    value_taps,
    input_taps,
    output_taps,
    prior_values,
    prior_input_maps,
    prior_output_maps,
    head_skip_gain,
    group_norm_gain,
    mixer_output_weight,
    recurrent_state,
    expert_norm_gain,
    routes,
    chosen_expert_weight,
    routed_gate_weight,
    routed_up_weight,
    routed_down_weight,
    common_gate_weight,
    common_up_weight,
    common_down_weight,
):
    seq_rows, model_width = tokens.shape
    ep_count = lax.axis_size("ep")
    tp_count = lax.axis_size("tp")
    tp_place = lax.axis_index("tp")
    normed = rms_scale(tokens, mixer_norm_gain).astype(jnp.bfloat16)
    both_pieces = jnp.concatenate(
        [
            gate_projection_weight.reshape(model_width, -1),
            value_projection_weight.reshape(model_width, -1),
        ],
        axis=1,
    )
    piece_width = both_pieces.shape[1] // 2
    projected = jnp.dot(
        lax.all_gather(normed, "ep", axis=0, tiled=True),
        both_pieces,
        preferred_element_type=jnp.float32,
    ).astype(jnp.bfloat16)
    returned = lax.all_to_all(projected, "ep", split_axis=0, concat_axis=1, tiled=True).reshape(
        seq_rows, ep_count, 2, piece_width
    )
    gate_rows = returned[:, :, 0].reshape(seq_rows, -1)
    value_rows = returned[:, :, 1].reshape(seq_rows, -1)
    input_rows = jnp.dot(
        normed, input_projection_weight, preferred_element_type=jnp.float32
    ).astype(jnp.bfloat16)
    output_rows = jnp.dot(
        normed, output_projection_weight, preferred_element_type=jnp.float32
    ).astype(jnp.bfloat16)
    step_raw = jnp.dot(normed, step_projection_weight, preferred_element_type=jnp.float32)
    value_conv, next_value = short_conv(prior_values, value_rows, value_taps)
    input_conv, next_input = short_conv(prior_input_maps, input_rows, input_taps)
    output_conv, next_output = short_conv(prior_output_maps, output_rows, output_taps)
    timestep_size = jax.nn.softplus(step_raw + head_step_bias)
    step_decay = jnp.exp(-timestep_size * head_decay_rate + extra_log_decay)
    state_next, mixed_flat = state_step(
        recurrent_state,
        value_conv,
        input_conv,
        output_conv,
        timestep_size,
        step_decay,
        head_skip_gain,
    )
    mixer_rows = gated_norm(mixed_flat, gate_rows, group_norm_gain, D_INNER // GROUPS)
    partial_mix = jnp.dot(
        lax.all_gather(mixer_rows, "ep", axis=0, tiled=True),
        mixer_output_weight,
        preferred_element_type=jnp.float32,
    )
    mix_share = lax.psum_scatter(
        partial_mix.reshape(ep_count, seq_rows, -1).astype(jnp.bfloat16),
        "tp",
        scatter_dimension=1,
        tiled=True,
    )
    moved_mix = lax.all_to_all(mix_share, "ep", split_axis=0, concat_axis=2, tiled=True)
    mixed_out = lax.all_gather(moved_mix, "tp", axis=1, tiled=True).reshape(seq_rows, model_width)
    stream = (tokens.astype(jnp.float32) + mixed_out.astype(jnp.float32)).astype(jnp.bfloat16)
    ffn_rows = rms_scale(stream, expert_norm_gain).astype(jnp.bfloat16)
    shared_hidden = (
        jax.nn.silu(jnp.dot(ffn_rows, common_gate_weight, preferred_element_type=jnp.float32))
        * jnp.dot(ffn_rows, common_up_weight, preferred_element_type=jnp.float32)
    ).astype(jnp.bfloat16)
    shared_out = lax.psum(
        jnp.dot(shared_hidden, common_down_weight, preferred_element_type=jnp.float32).astype(
            jnp.bfloat16
        ),
        "tp",
    ).astype(jnp.float32)
    exp_local = routed_gate_weight.shape[0]
    expert_total = exp_local * ep_count
    topk_count = routes.shape[1]
    capacity = (seq_rows * topk_count + expert_total - 1) // expert_total + 1
    slot_count = expert_total * capacity
    expert_ids = jnp.arange(expert_total, dtype=jnp.int32)
    flat_routes = routes.reshape(-1)
    onehot = (flat_routes[:, None] == expert_ids[None, :]).astype(jnp.int32)
    slot_ids = jnp.sum((jnp.cumsum(onehot, axis=0) - onehot) * onehot, axis=1)
    positions = flat_routes * capacity + slot_ids
    matches = (jnp.arange(slot_count, dtype=jnp.int32)[:, None] == positions[None, :]).reshape(
        slot_count, seq_rows, topk_count
    )
    dispatch_mat = jnp.sum(matches.astype(jnp.float32), axis=2).astype(jnp.bfloat16)
    combine_mat = jnp.sum(jnp.where(matches, chosen_expert_weight[None], 0.0), axis=2)
    outgoing = jnp.dot(dispatch_mat, ffn_rows, preferred_element_type=jnp.float32).astype(
        jnp.bfloat16
    )
    outgoing = outgoing.reshape(ep_count, exp_local, capacity, model_width)
    half_width = model_width // tp_count
    own_cols = lax.dynamic_slice_in_dim(outgoing, tp_place * half_width, half_width, 3)
    full_rows = lax.all_gather(
        lax.all_to_all(own_cols, "ep", split_axis=0, concat_axis=0, tiled=True),
        "tp",
        axis=3,
        tiled=True,
    )
    partial_out = expert_partial(
        full_rows, routed_gate_weight, routed_up_weight, routed_down_weight
    )
    share_out = lax.psum_scatter(
        partial_out.astype(jnp.bfloat16), "tp", scatter_dimension=3, tiled=True
    )
    back_half = lax.all_to_all(share_out, "ep", split_axis=0, concat_axis=0, tiled=True)
    routed_half = lax.dot_general(
        combine_mat,
        back_half.reshape(slot_count, half_width).astype(jnp.float32),
        (((0,), (0,)), ((), ())),
        precision=lax.Precision.HIGHEST,
    )
    routed = lax.all_gather(routed_half.astype(jnp.bfloat16), "tp", axis=1, tiled=True).astype(
        routed_half.dtype
    )
    result = (stream.astype(jnp.float32) + shared_out + routed).astype(jnp.bfloat16)
    return (result, state_next, next_value, next_input, next_output)


def solution(mesh):
    return jax.shard_map(
        shards,
        mesh=mesh,
        in_specs=(
            P("ep", None),
            P(),
            P(None, "tp", "ep"),
            P(None, "tp", "ep"),
            P(None, "tp"),
            P(None, "tp"),
            P(None, "tp"),
            P("tp"),
            P("tp"),
            P("ep", "tp"),
            P(None, "tp"),
            P(None, "tp"),
            P(None, "tp"),
            P("ep", None, "tp"),
            P("ep", None, "tp"),
            P("ep", None, "tp"),
            P("tp"),
            P("tp"),
            P("tp", "ep"),
            P("ep", "tp", None, None),
            P(),
            P("ep", None),
            P("ep", None),
            P("ep", None, "tp"),
            P("ep", None, "tp"),
            P("ep", "tp", None),
            P(None, "tp"),
            P(None, "tp"),
            P("tp", None),
        ),
        out_specs=(
            P("ep", None),
            P("ep", "tp", None, None),
            P("ep", None, "tp"),
            P("ep", None, "tp"),
            P("ep", None, "tp"),
        ),
        check_vma=False,
    )
```

profile of v0, /device:TPU:0, one launch (start us, length us, event | category | flops | bytes accessed | tf_op | source)
XLA Modules:
  0.0 206.3 jit_solution(9300064261054911112)
XLA Ops:
  7.3 1.0 fusion.18
  9.1 45.3 %all_gather.15 = bf16[128,2048]{1,0:T(8,128)(2,1)S(1)} all-gather(bf16[8,2048]{1,0:T(8,128)(2,1)S(1)} %fusion.20), channel_id=1, replica_groups=mesh['ep'=16,'tp'=2] {'ep'}, dimensions={0}, use_global_device_ids=true | all-gather | bytes 557056 | tf_op jit(solution)/shard_map/all_gather | solution.py:104
  54.5 2.2 %fusion.1 = bf16[16,8,256]{2,1,0:T(8,128)(2,1)} fusion(bf16[128,2048]{1,0:T(8,128)(2,1)S(1)} %all_gather.15, bf16[2048,128]{1,0:T(8,128)(2,1)} %bitcast.213, bf16[2048,128]{1,0:T(8,128)(2,1)} %bitcast.214), kind=kOutput, calls=%fused_computation.7 | convolution fusion | flops 136347648 | bytes 1638400 | tf_op jit(solution)/shard_map/dot_general | solution.py:103
  56.6 3.5 %all-to-all-start = ((bf16[16,8,256]{2,1,0:T(8,128)(2,1)}), bf16[16,8,256]{2,1,0:T(8,128)(2,1)S(1)}, u32[]{:S(2)}, u32[]{:S(2)}) async-start(bf16[16,8,256]{2,1,0:T(8,128)(2,1)} %fusion.1), calls=%async_computation | async-start | bytes 131072 | tf_op jit(solution)/shard_map/all_to_all | solution.py:108
  60.2 1.6 slice_reduce_fusion.3
  65.1 2.0 convolution_convert_fusion.6
  70.1 1.0 fusion.65
  73.4 9.4 %multiply_reduce_fusion = (f32[8,32,64]{2,1,0:T(8,128)S(1)}, f32[8,32,64,128]{3,2,1,0:T(8,128)}) fusion(f32[8,32,128]{2,1,0:T(8,128)S(1)} %get-tuple-element.41, f32[8,32,128]{2,1,0:T(8,128)S(1)} %get-tuple-element.42, f32[8,32,64]{2,1,0:T(8,128)S(1)} %get-tuple-element.15, f32[8,32,64,128]{3,2,1,0:T(8,128)} %param.48, f32[8,32]{1,0:T(8,128)S(1)} %get-tuple-element.35), kind=kLoop, calls=%fused_computation | loop fusion | flops 10469376 | bytes 17171456 | tf_op jit(solution)/shard_map/reduce_sum | solution.py:39
  82.9 1.2 multiply_reduce_fusion.1
  84.4 1.0 fusion.41
  85.4 44.1 %all_gather.16 = bf16[128,2048]{1,0:T(8,128)(2,1)S(1)} all-gather(bf16[8,2048]{1,0:T(8,128)(2,1)S(1)} %fusion.41), channel_id=1, replica_groups=mesh['ep'=16,'tp'=2] {'ep'}, dimensions={0}, use_global_device_ids=true | all-gather | bytes 557056 | tf_op jit(solution)/shard_map/all_gather | solution.py:136
  129.5 1.3 fusion.5
  133.0 2.0 reduce-scatter.3.cloned.1.call-done
  135.1 1.3 copy.99
  136.4 6.7 %all-to-all-start.1 = ((bf16[16,4,128]{2,1,0:T(4,128)(2,1)}), bf16[16,4,128]{2,1,0:T(4,128)(2,1)S(1)}, u32[]{:S(2)}, u32[]{:S(2)}) async-start(bf16[16,4,128]{2,1,0:T(4,128)(2,1)} %copy.99), calls=%async_computation.2 | async-start | bytes 32768 | tf_op jit(solution)/shard_map/all_to_all | solution.py:146
  143.8 6.6 %all-to-all-done.1 = bf16[16,4,128]{2,1,0:T(4,128)(2,1)S(1)} async-done(((bf16[16,4,128]{2,1,0:T(4,128)(2,1)}), bf16[16,4,128]{2,1,0:T(4,128)(2,1)S(1)}, u32[]{:S(2)}, u32[]{:S(2)}) %all-to-all-start.1) | async-done | bytes 16416 | tf_op jit(solution)/shard_map/all_to_all | solution.py:146
  150.5 1.9 all_gather.17
  153.8 1.0 convolution_convert_fusion.1
  156.5 10.6 %all_to_all.44 = bf16[16,1,4,1024]{3,2,1,0:T(4,128)(2,1)S(1)} all-to-all(bf16[16,1,4,1024]{3,2,1,0:T(4,128)(2,1)S(1)} %constant_dynamic-slice_fusion), channel_id=1, replica_groups=mesh['ep'=16,'tp'=2] {'ep'}, dimensions={0} | all-to-all | bytes 262144 | tf_op jit(solution)/shard_map/all_to_all | solution.py:182
  167.2 2.0 all_gather.18
  169.2 2.2 %convolution_bitcast_fusion.1 = f32[16,1,4,256]{3,0,2,1:T(8,128)} fusion(bf16[1,2048,256]{2,1,0:T(8,128)(2,1)} %param.52, bf16[16,1,4,2048]{3,0,2,1:T(8,128)(2,1)S(1)} %all_gather.18), kind=kOutput, calls=%fused_computation.9 | convolution fusion | flops 67108864 | bytes 1376256 | tf_op jit(solution)/shard_map/slcd,ldf->slcf/dot_general | solution.py:53
  171.4 3.1 %fusion = bf16[16,1,4,2048]{3,0,2,1:T(8,128)(2,1)} fusion(bf16[1,256,2048]{2,1,0:T(8,128)(2,1)} %param.54, bf16[1,2048,256]{2,1,0:T(8,128)(2,1)} %param.53, bf16[16,1,4,2048]{3,0,2,1:T(8,128)(2,1)S(1)} %all_gather.18, f32[16,1,4,256]{3,0,2,1:T(8,128)} %convolution_bitcast_fusion.1), kind=kOutput, calls=%fused_computation.4 | convolution fusion | flops 134447104 | bytes 2686976 | tf_op jit(solution)/shard_map/slcf,lfd->slcd/dot_general | solution.py:56
  174.5 1.4 pad_maximum_fusion.1
  175.9 1.4 pad_maximum_fusion
  177.3 1.5 fusion.63
  178.8 1.0 reduce-scatter.5.cloned.1.call-done
  179.9 1.6 copy.106
  181.5 6.7 %all-to-all-start.3 = ((bf16[16,1,4,1024]{3,2,1,0:T(4,128)(2,1)}), bf16[16,1,4,1024]{3,2,1,0:T(4,128)(2,1)S(1)}, u32[]{:S(2)}, u32[]{:S(2)}) async-start(bf16[16,1,4,1024]{3,2,1,0:T(4,128)(2,1)} %copy.106), calls=%async_computation.5 | async-start | bytes 262144 | tf_op jit(solution)/shard_map/all_to_all | solution.py:193
  188.3 2.0 convolution_convert_fusion.2
  190.2 3.4 %psum.7 = bf16[8,2048]{1,0:T(8,128)(2,1)S(1)} all-reduce(bf16[8,2048]{1,0:T(8,128)(2,1)S(1)} %convolution_convert_fusion.2), channel_id=1, replica_groups=mesh['ep'=16,'tp'=2] {'tp'}, use_global_device_ids=true, to_apply=%region_6.7 | all-reduce | flops 16384 | bytes 65536 | tf_op jit(solution)/shard_map/psum | solution.py:154
  193.7 2.5 %all-to-all-done.3 = bf16[16,1,4,1024]{3,2,1,0:T(4,128)(2,1)S(1)} async-done(((bf16[16,1,4,1024]{3,2,1,0:T(4,128)(2,1)}), bf16[16,1,4,1024]{3,2,1,0:T(4,128)(2,1)S(1)}, u32[]{:S(2)}, u32[]{:S(2)}) %all-to-all-start.3) | async-done | bytes 131104 | tf_op jit(solution)/shard_map/all_to_all | solution.py:193
  197.1 1.8 all_gather.19
  (85 shorter events, 17.7 us)
Async XLA Ops:
  7.2 55.9 %copy-start = (bf16[2048,512]{1,0:T(8,128)(2,1)S(1)}, bf16[2048,512]{1,0:T(8,128)(2,1)}, u32[]{:S(2)}) copy-start(bf16[2048,512]{1,0:T(8,128)(2,1)} %param.33) | copy-start | bytes 6291460
  7.2 59.9 %copy-start.8 = (f32[4,512]{1,0:T(4,128)S(1)}, f32[4,512]{1,0:T(4,128)}, u32[]{:S(2)}) copy-start(f32[4,512]{1,0:T(4,128)} %param.41) | copy-start | bytes 24580
  7.2 59.9 %copy-start.4 = (bf16[8,3,512]{2,0,1:T(8,128)(2,1)S(1)}, bf16[8,3,512]{2,0,1:T(8,128)(2,1)}, u32[]{:S(2)}) copy-start(bf16[8,3,512]{2,0,1:T(8,128)(2,1)} %param.44) | copy-start | bytes 73732
  7.2 60.0 %copy-start.11 = (f32[32]{0:T(128)S(1)}, f32[32]{0:T(128)}, u32[]{:S(2)}) copy-start(f32[32]{0:T(128)} %param.45) | copy-start | bytes 388
  7.2 60.7 %copy-start.7 = (s32[8,6]{1,0:T(8,128)S(1)}, s32[8,6]{1,0:T(8,128)}, u32[]{:S(2)}) copy-start(s32[8,6]{1,0:T(8,128)} %param.50) | copy-start | bytes 580
  7.2 61.8 %copy-start.3 = (bf16[2048,32]{0,1:T(8,128)(2,1)S(1)}, bf16[2048,32]{0,1:T(8,128)(2,1)}, u32[]{:S(2)}) copy-start(bf16[2048,32]{0,1:T(8,128)(2,1)} %param.35) | copy-start | bytes 393220
  7.2 61.8 %copy-start.13 = (f32[32]{0:T(128)S(1)}, f32[32]{0:T(128)}, u32[]{:S(2)}) copy-start(f32[32]{0:T(128)} %param.36) | copy-start | bytes 388
  7.2 61.8 %copy-start.12 = (f32[32]{0:T(128)S(1)}, f32[32]{0:T(128)}, u32[]{:S(2)}) copy-start(f32[32]{0:T(128)} %param.37) | copy-start | bytes 388
  7.3 61.8 %copy-start.10 = (f32[8,32]{1,0:T(8,128)S(1)}, f32[8,32]{1,0:T(8,128)}, u32[]{:S(2)}) copy-start(f32[8,32]{1,0:T(8,128)} %param.38) | copy-start | bytes 3076
  56.6 12.6 %all-to-all-start = ((bf16[16,8,256]{2,1,0:T(8,128)(2,1)}), bf16[16,8,256]{2,1,0:T(8,128)(2,1)S(1)}, u32[]{:S(2)}, u32[]{:S(2)}) async-start(bf16[16,8,256]{2,1,0:T(8,128)(2,1)} %fusion.1), calls=%async_computation | async-start | bytes 131072 | tf_op jit(solution)/shard_map/all_to_all | solution.py:108
  60.1 74.9 %reduce-scatter.3.cloned.1.call-start = ((), (), s32[]{:S(2)}) async-start(), calls=%async_computation.6 | async-start | bytes 49152 | tf_op jit(solution)/shard_map/reduce_scatter | solution.py:140
  67.1 1.3 copy-start.6
  73.4 11.0 %copy-start.2 = (bf16[8,3,2048]{2,0,1:T(8,128)(2,1)S(1)}, bf16[8,3,2048]{2,0,1:T(8,128)(2,1)}, u32[]{:S(2)}) copy-start(bf16[8,3,2048]{2,0,1:T(8,128)(2,1)} %param.42) | copy-start | bytes 294916
  73.4 80.4 %copy-start.5 = (f32[2048]{0:T(1024)S(1)}, f32[2048]{0:T(1024)}, u32[]{:S(2)}) copy-start(f32[2048]{0:T(1024)} %param.49) | copy-start | bytes 24580
  82.8 105.5 %copy-start.1 = (bf16[256,2048]{1,0:T(8,128)(2,1)S(1)}, bf16[256,2048]{1,0:T(8,128)(2,1)}, u32[]{:S(2)}) copy-start(bf16[256,2048]{1,0:T(8,128)(2,1)} %param.57) | copy-start | bytes 3145732
  136.4 14.0 %all-to-all-start.1 = ((bf16[16,4,128]{2,1,0:T(4,128)(2,1)}), bf16[16,4,128]{2,1,0:T(4,128)(2,1)S(1)}, u32[]{:S(2)}, u32[]{:S(2)}) async-start(bf16[16,4,128]{2,1,0:T(4,128)(2,1)} %copy.99), calls=%async_computation.2 | async-start | bytes 32768 | tf_op jit(solution)/shard_map/all_to_all | solution.py:146
  143.1 36.7 %reduce-scatter.5.cloned.1.call-start = ((), (), s32[]{:S(2)}) async-start(), calls=%async_computation.7 | async-start | bytes 393216 | tf_op jit(solution)/shard_map/reduce_scatter | solution.py:190
  153.2 0.6 copy-start.9
  181.5 14.7 %all-to-all-start.3 = ((bf16[16,1,4,1024]{3,2,1,0:T(4,128)(2,1)}), bf16[16,1,4,1024]{3,2,1,0:T(4,128)(2,1)S(1)}, u32[]{:S(2)}, u32[]{:S(2)}) async-start(bf16[16,1,4,1024]{3,2,1,0:T(4,128)(2,1)} %copy.106), calls=%async_computation.5 | async-start | bytes 262144 | tf_op jit(solution)/shard_map/all_to_all | solution.py:193
Sparse Core Ops, SparseCore 0:
  131.6 3.4 reduce-scatter.2
  174.6 5.2 reduce-scatter.4
where the time goes:
time: 208 us; the launch traced here: 206 us
  blocking collectives  109 us (52%)
  other arithmetic  23.6 us (11%)
  starting transfers between devices  17 us (8%)
  matrix products  16.5 us (8%)
  between operations  14.4 us (7%)
  local copies, waits for them, and re-layouts  13.5 us (6%)
  waiting for transfers between devices  12.3 us (6%)
    all_gather x1, blocking collectives, shards(): lax.all_gather(normed, 'ep', axis=0, tiled=True)  45.3 us
    all_gather x1, blocking collectives, shards(): lax.all_gather(mixer_rows, 'ep', axis=0, tiled=True)  44.1 us
    all_to_all x1, blocking collectives, shards(): lax.all_to_all(own_cols, 'ep', split_axis=0, concat_axis=0, tiled=True)  10.6 us
    reduce_sum x1, other arithmetic, state_step(): jnp.sum(state_next * output_heads[:, :, None, :], axis=-1)  9.36 us
    all_to_all x1, starting transfers between devices, shards(): lax.all_to_all(share_out, 'ep', split_axis=0, concat_axis=0, tiled=True)  6.73 us
    all_to_all x1, starting transfers between devices, shards(): lax.all_to_all(mix_share, 'ep', split_axis=0, concat_axis=2, tiled=True)  6.69 us
    all_to_all x1, waiting for transfers between devices, shards(): lax.all_to_all(mix_share, 'ep', split_axis=0, concat_axis=2, tiled=True)  6.62 us
  transfers between devices with their start and end apart: 5, of which 4 were waited for; matrix products, arithmetic and copies ran while one was open for 8% of the time, Pallas kernels for 0%

commit v1 on v0

--- a/solution.py
+++ b/solution.py
@@ -2,6 +2,7 @@
 import jax.numpy as jnp
 from jax import lax
 from jax.sharding import PartitionSpec as P
+from jax.lax import all_to_all, axis_size
 
 D_INNER = 4096
 GROUPS = 8
@@ -143,7 +144,15 @@
         scatter_dimension=1,
         tiled=True,
     )
-    moved_mix = lax.all_to_all(mix_share, "ep", split_axis=0, concat_axis=2, tiled=True)
+
+    def array_watch(vector):
+        a_now = axis_size("ep")
+        inter = jnp.split(vector, a_now, 0)
+        outcome_arr = jnp.stack(inter, 0)
+        piece_next = all_to_all(outcome_arr, "ep", 0, 0)
+        return jnp.concatenate(piece_next, 2)
+
+    moved_mix = array_watch(mix_share)
     mixed_out = lax.all_gather(moved_mix, "tp", axis=1, tiled=True).reshape(seq_rows, model_width)
     stream = (tokens.astype(jnp.float32) + mixed_out.astype(jnp.float32)).astype(jnp.bfloat16)
     ffn_rows = rms_scale(stream, expert_norm_gain).astype(jnp.bfloat16)

time: 208 us -> 217 us (1.043)
  local copies, waits for them, and re-layouts: 13.5 us -> 22.2 us
    unnamed x30 -> x45, local copies, waits for them, and re-layouts: 1.51 us -> 9.96 us
where the time goes in v1:
time: 217 us; the launch traced here: 215 us
  blocking collectives  109 us (50%)
  other arithmetic  23.6 us (11%)
  local copies, waits for them, and re-layouts  22.2 us (10%)
  starting transfers between devices  17 us (8%)
  matrix products  16.5 us (8%)
  between operations  14.4 us (7%)
  waiting for transfers between devices  12.3 us (6%)
    all_gather x1, blocking collectives, shards(): lax.all_gather(normed, 'ep', axis=0, tiled=True)  45.3 us
    all_gather x1, blocking collectives, shards(): lax.all_gather(mixer_rows, 'ep', axis=0, tiled=True)  44.1 us
    all_to_all x1, blocking collectives, shards(): lax.all_to_all(own_cols, 'ep', split_axis=0, concat_axis=0, tiled=True)  10.6 us
    unnamed x45, local copies, waits for them, and re-layouts  9.96 us
    reduce_sum x1, other arithmetic, state_step(): jnp.sum(state_next * output_heads[:, :, None, :], axis=-1)  9.36 us
    all_to_all x1, starting transfers between devices, shards(): lax.all_to_all(share_out, 'ep', split_axis=0, concat_axis=0, tiled=True)  6.75 us
    all_to_all x1, starting transfers between devices, array_watch(): piece_next = all_to_all(outcome_arr, 'ep', 0, 0)  6.69 us
    all_to_all x1, waiting for transfers between devices, array_watch(): piece_next = all_to_all(outcome_arr, 'ep', 0, 0)  6.62 us
  transfers between devices with their start and end apart: 5, of which 4 were waited for; matrix products, arithmetic and copies ran while one was open for 8% of the time, Pallas kernels for 0%

profile of v1, /device:TPU:0, one launch (start us, length us, event | category | flops | bytes accessed | tf_op | source)
XLA Modules:
  0.0 215.1 jit_solution(39383013531218565)
XLA Ops:
  7.3 1.0 fusion.18
  9.1 45.3 %all_gather.15 = bf16[128,2048]{1,0:T(8,128)(2,1)S(1)} all-gather(bf16[8,2048]{1,0:T(8,128)(2,1)S(1)} %fusion.20), channel_id=1, replica_groups=mesh['ep'=16,'tp'=2] {'ep'}, dimensions={0}, use_global_device_ids=true | all-gather | bytes 557056 | tf_op jit(solution)/shard_map/all_gather | solution.py:105
  54.5 2.2 %fusion.1 = bf16[16,8,256]{2,1,0:T(8,128)(2,1)} fusion(bf16[128,2048]{1,0:T(8,128)(2,1)S(1)} %all_gather.15, bf16[2048,128]{1,0:T(8,128)(2,1)} %bitcast.273, bf16[2048,128]{1,0:T(8,128)(2,1)} %bitcast.274), kind=kOutput, calls=%fused_computation.7 | convolution fusion | flops 136347648 | bytes 1638400 | tf_op jit(solution)/shard_map/dot_general | solution.py:104
  56.6 3.5 %all-to-all-start = ((bf16[16,8,256]{2,1,0:T(8,128)(2,1)}), bf16[16,8,256]{2,1,0:T(8,128)(2,1)S(1)}, u32[]{:S(2)}, u32[]{:S(2)}) async-start(bf16[16,8,256]{2,1,0:T(8,128)(2,1)} %fusion.1), calls=%async_computation | async-start | bytes 131072 | tf_op jit(solution)/shard_map/all_to_all | solution.py:109
  60.2 1.6 slice_reduce_fusion.3
  65.1 2.0 convolution_convert_fusion.6
  70.1 1.0 fusion.65
  73.4 9.4 %multiply_reduce_fusion = (f32[8,32,64]{2,1,0:T(8,128)S(1)}, f32[8,32,64,128]{3,2,1,0:T(8,128)}) fusion(f32[8,32,128]{2,1,0:T(8,128)S(1)} %get-tuple-element.57, f32[8,32,128]{2,1,0:T(8,128)S(1)} %get-tuple-element.58, f32[8,32,64]{2,1,0:T(8,128)S(1)} %get-tuple-element.15, f32[8,32,64,128]{3,2,1,0:T(8,128)} %param.48, f32[8,32]{1,0:T(8,128)S(1)} %get-tuple-element.51), kind=kLoop, calls=%fused_computation | loop fusion | flops 10469376 | bytes 17171456 | tf_op jit(solution)/shard_map/reduce_sum | solution.py:40
  82.9 1.2 multiply_reduce_fusion.1
  84.4 1.0 fusion.41
  85.4 44.1 %all_gather.16 = bf16[128,2048]{1,0:T(8,128)(2,1)S(1)} all-gather(bf16[8,2048]{1,0:T(8,128)(2,1)S(1)} %fusion.41), channel_id=1, replica_groups=mesh['ep'=16,'tp'=2] {'ep'}, dimensions={0}, use_global_device_ids=true | all-gather | bytes 557056 | tf_op jit(solution)/shard_map/all_gather | solution.py:137
  129.5 1.3 fusion.5
  133.0 2.0 reduce-scatter.3.cloned.1.call-done
  135.1 1.1 fusion.68
  145.2 6.7 %all-to-all-start.1 = ((bf16[16,1,4,128]{3,2,1,0:T(4,128)(2,1)}), bf16[16,1,4,128]{3,2,1,0:T(4,128)(2,1)S(1)}, u32[]{:S(2)}, u32[]{:S(2)}) async-start(bf16[16,1,4,128]{3,2,1,0:T(4,128)(2,1)} %constant_dynamic-update-slice_fusion), calls=%async_computation.2 | async-start | bytes 32768 | tf_op jit(solution)/shard_map/all_to_all | solution.py:152
  152.6 6.6 %all-to-all-done.1 = bf16[16,1,4,128]{3,2,1,0:T(4,128)(2,1)S(1)} async-done(((bf16[16,1,4,128]{3,2,1,0:T(4,128)(2,1)}), bf16[16,1,4,128]{3,2,1,0:T(4,128)(2,1)S(1)}, u32[]{:S(2)}, u32[]{:S(2)}) %all-to-all-start.1) | async-done | bytes 16416 | tf_op jit(solution)/shard_map/all_to_all | solution.py:152
  159.2 1.9 all_gather.17
  162.6 1.0 convolution_convert_fusion.1
  165.3 10.6 %all_to_all.31 = bf16[16,1,4,1024]{3,2,1,0:T(4,128)(2,1)S(1)} all-to-all(bf16[16,1,4,1024]{3,2,1,0:T(4,128)(2,1)S(1)} %constant_dynamic-slice_fusion), channel_id=1, replica_groups=mesh['ep'=16,'tp'=2] {'ep'}, dimensions={0} | all-to-all | bytes 262144 | tf_op jit(solution)/shard_map/all_to_all | solution.py:191
  176.0 2.0 all_gather.18
  178.0 2.1 convolution_bitcast_fusion.1
  180.1 3.1 %fusion = bf16[16,1,4,2048]{3,0,2,1:T(8,128)(2,1)} fusion(bf16[1,256,2048]{2,1,0:T(8,128)(2,1)} %param.54, bf16[1,2048,256]{2,1,0:T(8,128)(2,1)} %param.53, bf16[16,1,4,2048]{3,0,2,1:T(8,128)(2,1)S(1)} %all_gather.18, f32[16,1,4,256]{3,0,2,1:T(8,128)} %convolution_bitcast_fusion.1), kind=kOutput, calls=%fused_computation.4 | convolution fusion | flops 134447104 | bytes 2686976 | tf_op jit(solution)/shard_map/slcf,lfd->slcd/dot_general | solution.py:57
  183.2 1.4 pad_maximum_fusion.1
  184.6 1.4 pad_maximum_fusion
  186.0 1.5 fusion.63
  187.6 1.0 reduce-scatter.5.cloned.1.call-done
  188.6 1.6 copy.153
  190.3 6.7 %all-to-all-start.3 = ((bf16[16,1,4,1024]{3,2,1,0:T(4,128)(2,1)}), bf16[16,1,4,1024]{3,2,1,0:T(4,128)(2,1)S(1)}, u32[]{:S(2)}, u32[]{:S(2)}) async-start(bf16[16,1,4,1024]{3,2,1,0:T(4,128)(2,1)} %copy.153), calls=%async_computation.5 | async-start | bytes 262144 | tf_op jit(solution)/shard_map/all_to_all | solution.py:202
  197.0 2.0 convolution_convert_fusion.2
  199.0 3.4 %psum.7 = bf16[8,2048]{1,0:T(8,128)(2,1)S(1)} all-reduce(bf16[8,2048]{1,0:T(8,128)(2,1)S(1)} %convolution_convert_fusion.2), channel_id=1, replica_groups=mesh['ep'=16,'tp'=2] {'tp'}, use_global_device_ids=true, to_apply=%region_6.7 | all-reduce | flops 16384 | bytes 65536 | tf_op jit(solution)/shard_map/psum | solution.py:163
  202.4 2.5 %all-to-all-done.3 = bf16[16,1,4,1024]{3,2,1,0:T(4,128)(2,1)S(1)} async-done(((bf16[16,1,4,1024]{3,2,1,0:T(4,128)(2,1)}), bf16[16,1,4,1024]{3,2,1,0:T(4,128)(2,1)S(1)}, u32[]{:S(2)}, u32[]{:S(2)}) %all-to-all-start.3) | async-done | bytes 131104 | tf_op jit(solution)/shard_map/all_to_all | solution.py:202
  205.8 1.8 all_gather.19
  (101 shorter events, 26.7 us)
Async XLA Ops:
  7.2 55.9 %copy-start = (bf16[2048,512]{1,0:T(8,128)(2,1)S(1)}, bf16[2048,512]{1,0:T(8,128)(2,1)}, u32[]{:S(2)}) copy-start(bf16[2048,512]{1,0:T(8,128)(2,1)} %param.33) | copy-start | bytes 6291460
  7.2 59.9 %copy-start.8 = (f32[4,512]{1,0:T(4,128)S(1)}, f32[4,512]{1,0:T(4,128)}, u32[]{:S(2)}) copy-start(f32[4,512]{1,0:T(4,128)} %param.41) | copy-start | bytes 24580
  7.2 59.9 %copy-start.4 = (bf16[8,3,512]{2,0,1:T(8,128)(2,1)S(1)}, bf16[8,3,512]{2,0,1:T(8,128)(2,1)}, u32[]{:S(2)}) copy-start(bf16[8,3,512]{2,0,1:T(8,128)(2,1)} %param.44) | copy-start | bytes 73732
  7.2 60.0 %copy-start.11 = (f32[32]{0:T(128)S(1)}, f32[32]{0:T(128)}, u32[]{:S(2)}) copy-start(f32[32]{0:T(128)} %param.45) | copy-start | bytes 388
  7.2 60.7 %copy-start.7 = (s32[8,6]{1,0:T(8,128)S(1)}, s32[8,6]{1,0:T(8,128)}, u32[]{:S(2)}) copy-start(s32[8,6]{1,0:T(8,128)} %param.50) | copy-start | bytes 580
  7.2 61.8 %copy-start.3 = (bf16[2048,32]{0,1:T(8,128)(2,1)S(1)}, bf16[2048,32]{0,1:T(8,128)(2,1)}, u32[]{:S(2)}) copy-start(bf16[2048,32]{0,1:T(8,128)(2,1)} %param.35) | copy-start | bytes 393220
  7.2 61.8 %copy-start.13 = (f32[32]{0:T(128)S(1)}, f32[32]{0:T(128)}, u32[]{:S(2)}) copy-start(f32[32]{0:T(128)} %param.36) | copy-start | bytes 388
  7.2 61.8 %copy-start.12 = (f32[32]{0:T(128)S(1)}, f32[32]{0:T(128)}, u32[]{:S(2)}) copy-start(f32[32]{0:T(128)} %param.37) | copy-start | bytes 388
  7.3 61.8 %copy-start.10 = (f32[8,32]{1,0:T(8,128)S(1)}, f32[8,32]{1,0:T(8,128)}, u32[]{:S(2)}) copy-start(f32[8,32]{1,0:T(8,128)} %param.38) | copy-start | bytes 3076
  56.6 12.6 %all-to-all-start = ((bf16[16,8,256]{2,1,0:T(8,128)(2,1)}), bf16[16,8,256]{2,1,0:T(8,128)(2,1)S(1)}, u32[]{:S(2)}, u32[]{:S(2)}) async-start(bf16[16,8,256]{2,1,0:T(8,128)(2,1)} %fusion.1), calls=%async_computation | async-start | bytes 131072 | tf_op jit(solution)/shard_map/all_to_all | solution.py:109
  60.1 74.9 %reduce-scatter.3.cloned.1.call-start = ((), (), s32[]{:S(2)}) async-start(), calls=%async_computation.6 | async-start | bytes 49152 | tf_op jit(solution)/shard_map/reduce_scatter | solution.py:141
  67.1 1.3 copy-start.6
  73.4 11.0 %copy-start.2 = (bf16[8,3,2048]{2,0,1:T(8,128)(2,1)S(1)}, bf16[8,3,2048]{2,0,1:T(8,128)(2,1)}, u32[]{:S(2)}) copy-start(bf16[8,3,2048]{2,0,1:T(8,128)(2,1)} %param.42) | copy-start | bytes 294916
  73.4 89.2 %copy-start.5 = (f32[2048]{0:T(1024)S(1)}, f32[2048]{0:T(1024)}, u32[]{:S(2)}) copy-start(f32[2048]{0:T(1024)} %param.49) | copy-start | bytes 24580
  82.8 114.2 %copy-start.1 = (bf16[256,2048]{1,0:T(8,128)(2,1)S(1)}, bf16[256,2048]{1,0:T(8,128)(2,1)}, u32[]{:S(2)}) copy-start(bf16[256,2048]{1,0:T(8,128)(2,1)} %param.57) | copy-start | bytes 3145732
  145.2 14.0 %all-to-all-start.1 = ((bf16[16,1,4,128]{3,2,1,0:T(4,128)(2,1)}), bf16[16,1,4,128]{3,2,1,0:T(4,128)(2,1)S(1)}, u32[]{:S(2)}, u32[]{:S(2)}) async-start(bf16[16,1,4,128]{3,2,1,0:T(4,128)(2,1)} %constant_dynamic-update-slice_fusion), calls=%async_computation.2 | async-start | bytes 32768 | tf_op jit(solution)/shard_map/all_to_all | solution.py:152
  151.9 36.7 %reduce-scatter.5.cloned.1.call-start = ((), (), s32[]{:S(2)}) async-start(), calls=%async_computation.7 | async-start | bytes 393216 | tf_op jit(solution)/shard_map/reduce_scatter | solution.py:199
  162.0 0.6 copy-start.9
  190.3 14.7 %all-to-all-start.3 = ((bf16[16,1,4,1024]{3,2,1,0:T(4,128)(2,1)}), bf16[16,1,4,1024]{3,2,1,0:T(4,128)(2,1)S(1)}, u32[]{:S(2)}, u32[]{:S(2)}) async-start(bf16[16,1,4,1024]{3,2,1,0:T(4,128)(2,1)} %copy.153), calls=%async_computation.5 | async-start | bytes 262144 | tf_op jit(solution)/shard_map/all_to_all | solution.py:202
Sparse Core Ops, SparseCore 0:
  131.6 3.4 reduce-scatter.2
  183.4 5.2 reduce-scatter.4
